TPU v7x, 32 devices: a whole 2x2x4 slice. The times are simulated.
32 devices in a mesh: sp: 16 (over z, y, x), tp: 2 (over core).
Axes of the slice: x: 2, y: 2, z: 4, core: 2. Of those that a mesh axis runs over, the one named last changes fastest.
Arguments:
- tokens: bfloat16 [4096, 2048], P('sp', 'tp'), may hold values from -24 to 24
- value_weight: bfloat16 [2, 2048, 2048], P(None, 'sp', 'tp'), may hold values from -0.125 to 0.125
- outer_weight: bfloat16 [2, 2048, 2048], P(None, 'sp', 'tp'), may hold values from -0.125 to 0.125
- inner_weight: bfloat16 [2, 2048, 2048], P(None, 'sp', 'tp'), may hold values from -0.125 to 0.125
- conv_taps: float32 [2, 3, 2048], P(None, None, 'tp'), may hold values from -3.5 to 3.5
- output_weight: bfloat16 [2, 2048, 2048], P(None, 'tp', 'sp'), may hold values from -2 to 2
- norm_gain: float32 [2, 2048], P(None, 'tp'), may hold values from 0.1 to 1.9
- norm_bias: float32 [2, 2048], P(None, 'tp'), may hold values from -3 to 3
Outputs:
- mixed_out: bfloat16 [4096, 2048], P('sp', 'tp')
All inputs are finite; a program needn't handle non-finite values.
Results may differ from a plain program's by a relative error of at most 0.03.
Values may be sent and summed in bfloat16 or wider, within the bound.
A program may use at most 64 MiB of HBM per device.

v0:
```python
import jax
import jax.numpy as jnp
from jax import lax
from jax.sharding import PartitionSpec as P

D = 2048
LAYERS = 2


def from_behind(array, axis, by):
    peers = lax.axis_size(axis)
    pairs = [(i, i + by) for i in range(peers) if 0 <= i + by < peers]
    return lax.ppermute(array, axis, pairs)


def input_products(whole, weights):
    return tuple(
        (
            jnp.dot(whole, weight, preferred_element_type=jnp.float32).astype(jnp.bfloat16)
            for weight in weights
        )
    )


def shards(
    tokens, value_weight, outer_weight, inner_weight, conv_taps, output_weight, norm_gain, norm_bias
):
    alpha = (2.0 * LAYERS) ** 0.25
    state = tokens
    taps_count = conv_taps.shape[1]
    all_value, all_outer, all_inner, all_output = (
        lax.all_gather(value_weight, "sp", axis=1, tiled=True),
        lax.all_gather(outer_weight, "sp", axis=1, tiled=True),
        lax.all_gather(inner_weight, "sp", axis=1, tiled=True),
        lax.all_gather(output_weight, "sp", axis=2, tiled=True),
    )
    for layer in range(LAYERS):
        whole = lax.all_gather(state, "tp", axis=1, tiled=True)
        u_part, outer, inner = input_products(
            whole, (all_value[layer], all_outer[layer], all_inner[layer])
        )
        gated_in = inner.astype(jnp.float32) * u_part.astype(jnp.float32)
        previous = from_behind(gated_in[gated_in.shape[0] - (taps_count - 1) :], "sp", 1)
        padded = jnp.concatenate([previous, gated_in], axis=0)
        conv = jnp.zeros_like(gated_in)
        for tap in range(taps_count):
            conv = conv + conv_taps[layer, tap][None, :] * padded[tap : tap + gated_in.shape[0]]
        gated = (outer.astype(jnp.float32) * conv).astype(jnp.bfloat16)
        terms = jnp.dot(gated, all_output[layer], preferred_element_type=jnp.float32)
        branch = lax.psum_scatter(
            terms.astype(jnp.bfloat16), "tp", scatter_dimension=1, tiled=True
        ).astype(jnp.float32)
        pre = alpha * state.astype(jnp.float32) + branch
        total, squares = lax.psum(
            (jnp.sum(pre, axis=-1, keepdims=True), jnp.sum(pre * pre, axis=-1, keepdims=True)), "tp"
        )
        mean = total / D
        var = jnp.maximum(squares / D - mean * mean, 0.0)
        normed = (pre - mean) * lax.rsqrt(var + 1e-05)
        state = (normed * norm_gain[layer][None, :] + norm_bias[layer][None, :]).astype(
            jnp.bfloat16
        )
    return state


def solution(mesh):
    in_specs = (
        P("sp", "tp"),
        P(None, "sp", "tp"),
        P(None, "sp", "tp"),
        P(None, "sp", "tp"),
        P(None, None, "tp"),
        P(None, "tp", "sp"),
        P(None, "tp"),
        P(None, "tp"),
    )
    out_specs = P("sp", "tp")
    return jax.shard_map(shards, mesh=mesh, in_specs=in_specs, out_specs=out_specs, check_vma=False)
```

profile of v0, /device:TPU:0, one launch (start us, length us, event | category | flops | bytes accessed | tf_op | source)
XLA Modules:
  0.0 578.4 jit_solution(5210033657117156722)
XLA Ops:
  6.5 0.7 all-gather.7.cloned.1.call-update
  10.0 10.7 %all-gather.7.cloned.1.call-done = bf16[256,2048]{1,0:T(8,128)(2,1)} async-done(((bf16[256,1024]{1,0:T(8,128)(2,1)}), bf16[256,2048]{1,0:T(8,128)(2,1)}) %all-gather.7.cloned.1.call-update) | async-done | bytes 1048592 | tf_op jit(solution)/shard_map/all_gather | solution.py:38
  20.7 116.2 %all-gather.13.cloned.1.call-done = bf16[2,2048,1024]{2,1,0:T(8,128)(2,1)} async-done(((bf16[2,128,1024]{2,1,0:T(8,128)(2,1)}), bf16[2,2048,1024]{2,1,0:T(8,128)(2,1)}) %all-gather.13.cloned.1.call-update) | async-done | bytes 8388624 | tf_op jit(solution)/shard_map/all_gather | solution.py:32
  136.8 4.7 fusion.16
  141.5 108.4 %all-gather.11.cloned.1.call-done = bf16[2,2048,1024]{2,1,0:T(8,128)(2,1)} async-done(((bf16[2,128,1024]{2,1,0:T(8,128)(2,1)}), bf16[2,2048,1024]{2,1,0:T(8,128)(2,1)}) %all-gather.11.cloned.1.call-update) | async-done | bytes 8388624 | tf_op jit(solution)/shard_map/all_gather | solution.py:34
  250.0 3.8 fusion.14
  253.8 3.4 collective-permute-start
  257.2 135.4 %all-gather.15.cloned.1.call-done = bf16[2,1024,2048]{2,1,0:T(8,128)(2,1)} async-done(((bf16[2,1024,128]{2,1,0:T(8,128)(2,1)}), bf16[2,1024,2048]{2,1,0:T(8,128)(2,1)}) %all-gather.15.cloned.1.call-update) | async-done | bytes 8388624 | tf_op jit(solution)/shard_map/all_gather | solution.py:35
  392.6 113.0 %all-gather.9.cloned.1.call-done = bf16[2,2048,1024]{2,1,0:T(8,128)(2,1)} async-done(((bf16[2,128,1024]{2,1,0:T(8,128)(2,1)}), bf16[2,2048,1024]{2,1,0:T(8,128)(2,1)}) %all-gather.9.cloned.1.call-update) | async-done | bytes 8388624 | tf_op jit(solution)/shard_map/all_gather | solution.py:33
  505.6 7.0 %fusion.8 = bf16[256,2048]{1,0:T(8,128)(2,1)} fusion(bf16[2,1024,2048]{2,1,0:T(8,128)(2,1)} %all-gather.15.cloned.1.call-done, f32[2,1024]{1,0:T(2,128)S(1)} %collective-permute-done, f32[256,1024]{1,0:T(8,128)S(1)} %fusion.14, bf16[256,2048]{1,0:T(8,128)(2,1)S(1)} %copy-done.5, bf16[2,2048,1024]{2,1,0:T(8,128)(2,1)} %all-gather.9.cloned.1.call-done, ...), kind=kOutput, calls=%fused_computation.16 | convolution fusion | flops 2150891520 | bytes 11554816 | tf_op jit(solution)/shard_map/dot_general | solution.py:49
  512.8 6.6 %reduce-scatter.3.cloned.1.call-done = bf16[256,1024]{1,0:T(8,128)(2,1)} async-done(((bf16[256,2048]{1,0:T(8,128)(2,1)}), bf16[256,1024]{1,0:T(8,128)(2,1)}) %reduce-scatter.3.cloned.1.call-update) | async-done | bytes 524304 | tf_op jit(solution)/shard_map/reduce_scatter | solution.py:50
  519.4 1.4 fusion.38
  520.8 2.5 all-reduce.1
  523.3 2.2 add_convert_fusion.1
  525.5 10.3 %all-gather.17.cloned.1.call-done = bf16[256,2048]{1,0:T(8,128)(2,1)} async-done(((bf16[256,1024]{1,0:T(8,128)(2,1)}), bf16[256,2048]{1,0:T(8,128)(2,1)}) %all-gather.17.cloned.1.call-update) | async-done | bytes 1048592 | tf_op jit(solution)/shard_map/all_gather | solution.py:38
  535.9 3.8 fusion.23
  539.7 3.5 fusion.21
  543.2 3.6 collective-permute-start.1
  546.9 1.3 collective-permute-done.1
  548.2 7.0 %fusion.9 = bf16[256,2048]{1,0:T(8,128)(2,1)} fusion(bf16[2,1024,2048]{2,1,0:T(8,128)(2,1)} %all-gather.15.cloned.1.call-done, f32[2,1024]{1,0:T(2,128)S(1)} %collective-permute-done.1, f32[256,1024]{1,0:T(8,128)S(1)} %fusion.21, bf16[256,2048]{1,0:T(8,128)(2,1)S(1)} %copy-done.6, bf16[2,2048,1024]{2,1,0:T(8,128)(2,1)} %all-gather.9.cloned.1.call-done, ...), kind=kOutput, calls=%fused_computation.17 | convolution fusion | flops 2150891520 | bytes 11554816 | tf_op jit(solution)/shard_map/dot_general | solution.py:49
  555.3 10.3 %reduce-scatter.5.cloned.1.call-done = bf16[256,1024]{1,0:T(8,128)(2,1)} async-done(((bf16[256,2048]{1,0:T(8,128)(2,1)}), bf16[256,1024]{1,0:T(8,128)(2,1)}) %reduce-scatter.5.cloned.1.call-update) | async-done | bytes 524304 | tf_op jit(solution)/shard_map/reduce_scatter | solution.py:50
  565.5 1.4 fusion.39
  566.9 2.5 all-reduce
  569.4 2.2 add_convert_fusion
  (37 shorter events, 2.9 us)
Async XLA Ops:
  6.5 14.1 %all-gather.7.cloned.1.call-start = ((), (), s32[]{:S(2)}) async-start(), calls=%async_computation.2 | async-start | bytes 1572864 | tf_op jit(solution)/shard_map/all_gather | solution.py:38
  7.3 129.6 %all-gather.13.cloned.1.call-start = ((), (), s32[]{:S(2)}) async-start(), calls=%async_computation.5 | async-start | bytes 8912896 | tf_op jit(solution)/shard_map/all_gather | solution.py:32
  8.0 242.0 %all-gather.11.cloned.1.call-start = ((), (), s32[]{:S(2)}) async-start(), calls=%async_computation.4 | async-start | bytes 8912896 | tf_op jit(solution)/shard_map/all_gather | solution.py:34
  8.7 383.9 %all-gather.15.cloned.1.call-start = ((), (), s32[]{:S(2)}) async-start(), calls=%async_computation.6 | async-start | bytes 8912896 | tf_op jit(solution)/shard_map/all_gather | solution.py:35
  9.3 496.3 %all-gather.9.cloned.1.call-start = ((), (), s32[]{:S(2)}) async-start(), calls=%async_computation.3 | async-start | bytes 8912896 | tf_op jit(solution)/shard_map/all_gather | solution.py:33
  9.9 247.2 %copy-start.2 = (f32[2,3,1024]{2,0,1:T(2,128)S(1)}, f32[2,3,1024]{2,0,1:T(2,128)}, u32[]{:S(2)}) copy-start(f32[2,3,1024]{2,0,1:T(2,128)} %param.12) | copy-start | bytes 73732
  9.9 509.5 %reduce-scatter.3.cloned.1.call-start = ((), (), s32[]{:S(2)}) async-start(), calls=%async_computation.7 | async-start | bytes 1572864 | tf_op jit(solution)/shard_map/reduce_scatter | solution.py:50
  20.7 229.3 %copy-start.5 = (bf16[256,2048]{1,0:T(8,128)(2,1)S(1)}, bf16[256,2048]{1,0:T(8,128)(2,1)}, u32[]{:S(2)}) copy-start(bf16[256,2048]{1,0:T(8,128)(2,1)} %all-gather.7.cloned.1.call-done) | copy-start | bytes 3145732
  253.8 251.9 %collective-permute-start = (f32[2,1024]{1,0:T(2,128)S(1)}, f32[2,1024]{1,0:T(2,128)S(1)}, u32[]{:S(2)}, u32[]{:S(2)}) collective-permute-start(f32[2,1024]{1,0:T(2,128)S(1)} %slice.99), channel_id=1, source_target_pairs={{0,2},{2,4},{4,6},{6,8},{8,10},{10,12},{12,14},{14,16},{16,18},{18... | collective-permute-start | bytes 24584 | tf_op jit(solution)/shard_map/ppermute | solution.py:13
  505.6 7.1 %copy-start.3 = (f32[2,1024]{1,0:T(2,128)S(1)}, f32[2,1024]{1,0:T(2,128)}, u32[]{:S(2)}) copy-start(f32[2,1024]{1,0:T(2,128)} %param.14) | copy-start | bytes 24580
  505.6 7.2 %copy-start.4 = (f32[2,1024]{1,0:T(2,128)S(1)}, f32[2,1024]{1,0:T(2,128)}, u32[]{:S(2)}) copy-start(f32[2,1024]{1,0:T(2,128)} %param.15) | copy-start | bytes 24580
  505.6 13.8 %copy-start.1 = (bf16[256,1024]{1,0:T(8,128)(2,1)S(1)}, bf16[256,1024]{1,0:T(8,128)(2,1)}, u32[]{:S(2)}) copy-start(bf16[256,1024]{1,0:T(8,128)(2,1)} %param.8) | copy-start | bytes 1572868
  512.7 23.1 %all-gather.17.cloned.1.call-start = ((), (), s32[]{:S(2)}) async-start(), calls=%async_computation.8 | async-start | bytes 1572864 | tf_op jit(solution)/shard_map/all_gather | solution.py:38
  525.5 40.1 %reduce-scatter.5.cloned.1.call-start = ((), (), s32[]{:S(2)}) async-start(), calls=%async_computation.9 | async-start | bytes 1572864 | tf_op jit(solution)/shard_map/reduce_scatter | solution.py:50
  535.9 3.8 copy-start.6
  543.2 5.0 collective-permute-start.1
  548.2 17.3 %copy-start = (bf16[256,1024]{1,0:T(8,128)(2,1)S(1)}, bf16[256,1024]{1,0:T(8,128)(2,1)}, u32[]{:S(2)}) copy-start(bf16[256,1024]{1,0:T(8,128)(2,1)} %add_convert_fusion.1) | copy-start | bytes 1572868
Sparse Core Ops, SparseCore 0:
  8.9 11.7 all-gather.6
  23.4 113.3 all-gather.12
  139.6 110.3 all-gather.10
  252.6 140.0 all-gather.14
  395.2 110.3 all-gather.8
  512.8 6.5 reduce-scatter.2
  525.6 10.2 all-gather.16
  555.4 10.0 reduce-scatter.4
where the time goes:
time: 579 us; the launch traced here: 578 us
  waiting for transfers between devices  515 us (89%)
  matrix products  29.9 us (5%)
  between operations  13.6 us (2%)
  starting transfers between devices  7.27 us (1%)
  other arithmetic  7.1 us (1%)
    all_gather x1, waiting for transfers between devices, shards(): lax.all_gather(output_weight, 'sp', axis=2, tiled=True)  135 us
    all_gather x1, waiting for transfers between devices, shards(): lax.all_gather(value_weight, 'sp', axis=1, tiled=True)  116 us
    all_gather x1, waiting for transfers between devices, shards(): lax.all_gather(outer_weight, 'sp', axis=1, tiled=True)  113 us
    all_gather x1, waiting for transfers between devices, shards(): lax.all_gather(inner_weight, 'sp', axis=1, tiled=True)  108 us
    all_gather x2, waiting for transfers between devices, shards(): whole = lax.all_gather(state, 'tp', axis=1, tiled=True)  21 us
    reduce_scatter x2, waiting for transfers between devices, shards(): lax.psum_scatter(terms.astype(jnp.bfloat16), 'tp', scatter_dimension=1, t...  16.9 us
    dot_general x4, matrix products, input_products(): jnp.dot(whole, weight, preferred_element_type=jnp.float32)  15.8 us
    dot_general x2, matrix products, shards(): jnp.dot(gated, all_output[layer], preferred_element_type=jnp.float32)  14.1 us
  transfers between devices with their start and end apart: 10, of which 9 were waited for; matrix products, arithmetic and copies ran while one was open for 1% of the time, Pallas kernels for 0%

commit v1 on v0

--- a/solution.py
+++ b/solution.py
@@ -29,7 +29,7 @@
     state = tokens
     taps_count = conv_taps.shape[1]
     all_value, all_outer, all_inner, all_output = (
-        lax.all_gather(value_weight, "sp", axis=1, tiled=True),
+        jnp.concatenate(lax.all_gather(value_weight, "sp"), axis=1),
         lax.all_gather(outer_weight, "sp", axis=1, tiled=True),
         lax.all_gather(inner_weight, "sp", axis=1, tiled=True),
         lax.all_gather(output_weight, "sp", axis=2, tiled=True),

time: 579 us -> 579 us (level)
  local copies, waits for them, and re-layouts: 0.08 us -> 6.27 us
  waiting for transfers between devices: 515 us -> 509 us
    all_gather x2, waiting for transfers between devices: 21 us -> 12.9 us  [shards(): whole = lax.all_gather(state, 'tp', axis=1, tiled=True)]
    all_gather x1, waiting for transfers between devices: 135 us -> 143 us  [shards(): lax.all_gather(output_weight, 'sp', axis=2, tiled=True)]
    all_gather x1, waiting for transfers between devices: 113 us -> 106 us  [shards(): lax.all_gather(outer_weight, 'sp', axis=1, tiled=True)]
    slice x0 -> x1, local copies, waits for them, and re-layouts: none -> 6.19 us  [shards(): all_value[layer]]
  transfers between devices with their start and end apart: 10 -> 10, of which waited for: 9 -> 9; matrix products, arithmetic and copies ran while one was open for 1% -> 3% of each run, Pallas kernels for 0% -> 0%
where the time goes in v1:
time: 579 us
  waiting for transfers between devices  509 us (88%)
  matrix products  30.2 us (5%)
  between operations  13.6 us (2%)
  starting transfers between devices  7.27 us (1%)
  other arithmetic  7.09 us (1%)
  local copies, waits for them, and re-layouts  6.27 us (1%)
    all_gather x1, waiting for transfers between devices, shards(): lax.all_gather(output_weight, 'sp', axis=2, tiled=True)  143 us
    all_gather x1, waiting for transfers between devices, shards(): lax.all_gather(value_weight, 'sp')  115 us
    all_gather x1, waiting for transfers between devices, shards(): lax.all_gather(inner_weight, 'sp', axis=1, tiled=True)  111 us
    all_gather x1, waiting for transfers between devices, shards(): lax.all_gather(outer_weight, 'sp', axis=1, tiled=True)  106 us
    reduce_scatter x2, waiting for transfers between devices, shards(): lax.psum_scatter(terms.astype(jnp.bfloat16), 'tp', scatter_dimension=1, t...  16.9 us
    dot_general x4, matrix products, input_products(): jnp.dot(whole, weight, preferred_element_type=jnp.float32)  16 us
    dot_general x2, matrix products, shards(): jnp.dot(gated, all_output[layer], preferred_element_type=jnp.float32)  14.1 us
    all_gather x2, waiting for transfers between devices, shards(): whole = lax.all_gather(state, 'tp', axis=1, tiled=True)  12.9 us
  transfers between devices with their start and end apart: 10, of which 9 were waited for; matrix products, arithmetic and copies ran while one was open for 3% of the time, Pallas kernels for 0%

profile of v1, /device:TPU:0, one launch (start us, length us, event | category | flops | bytes accessed | tf_op | source)
XLA Modules:
  0.0 578.6 jit_solution(6971229221123413728)
XLA Ops:
  10.0 115.2 %all-gather.18.cloned.1.call-done = bf16[32,128,1024]{2,1,0:T(8,128)(2,1)} async-done(((bf16[2,128,1024]{2,1,0:T(8,128)(2,1)}), bf16[32,128,1024]{2,1,0:T(8,128)(2,1)}) %all-gather.18.cloned.1.call-update) | async-done | bytes 8388624 | tf_op jit(solution)/shard_map/all_gather | solution.py:32
  125.2 6.2 %fusion.46 = (bf16[1,16,128,1024]{3,2,0,1:T(8,128)(2,1)}, bf16[1,16,128,1024]{3,2,0,1:T(8,128)(2,1)}) fusion(bf16[2,16,128,1024]{3,2,0,1:T(8,128)(2,1)} %bitcast.81), kind=kLoop, calls=%fused_computation.68 | loop fusion | bytes 16777216 | tf_op jit(solution)/shard_map/slice | solution.py:40
  131.4 2.6 all-gather.8.cloned.1.call-done
  133.9 4.9 fusion.19
  138.8 111.3 %all-gather.12.cloned.1.call-done = bf16[2,2048,1024]{2,1,0:T(8,128)(2,1)} async-done(((bf16[2,128,1024]{2,1,0:T(8,128)(2,1)}), bf16[2,2048,1024]{2,1,0:T(8,128)(2,1)}) %all-gather.12.cloned.1.call-update) | async-done | bytes 8388624 | tf_op jit(solution)/shard_map/all_gather | solution.py:34
  250.1 3.8 fusion.12
  253.9 3.4 collective-permute-start
  257.3 105.8 %all-gather.10.cloned.1.call-done = bf16[2,2048,1024]{2,1,0:T(8,128)(2,1)} async-done(((bf16[2,128,1024]{2,1,0:T(8,128)(2,1)}), bf16[2,2048,1024]{2,1,0:T(8,128)(2,1)}) %all-gather.10.cloned.1.call-update) | async-done | bytes 8388624 | tf_op jit(solution)/shard_map/all_gather | solution.py:33
  363.1 142.6 %all-gather.14.cloned.1.call-done = bf16[2,1024,2048]{2,1,0:T(8,128)(2,1)} async-done(((bf16[2,1024,128]{2,1,0:T(8,128)(2,1)}), bf16[2,1024,2048]{2,1,0:T(8,128)(2,1)}) %all-gather.14.cloned.1.call-update) | async-done | bytes 8388624 | tf_op jit(solution)/shard_map/all_gather | solution.py:35
  505.7 7.1 %fusion.6 = bf16[256,2048]{1,0:T(8,128)(2,1)} fusion(bf16[2,1024,2048]{2,1,0:T(8,128)(2,1)} %all-gather.14.cloned.1.call-done, f32[2,1024]{1,0:T(2,128)S(1)} %collective-permute-done, f32[256,1024]{1,0:T(8,128)S(1)} %fusion.12, bf16[256,2048]{1,0:T(8,128)(2,1)S(1)} %copy-done.5, bf16[2,2048,1024]{2,1,0:T(8,128)(2,1)} %all-gather.10.cloned.1.call-done, ...), kind=kOutput, calls=%fused_computation.12 | convolution fusion | flops 2150891520 | bytes 11554816 | tf_op jit(solution)/shard_map/dot_general | solution.py:49
  513.0 6.6 %reduce-scatter.3.cloned.1.call-done = bf16[256,1024]{1,0:T(8,128)(2,1)} async-done(((bf16[256,2048]{1,0:T(8,128)(2,1)}), bf16[256,1024]{1,0:T(8,128)(2,1)}) %reduce-scatter.3.cloned.1.call-update) | async-done | bytes 524304 | tf_op jit(solution)/shard_map/reduce_scatter | solution.py:50
  519.6 1.4 fusion.34
  521.0 2.5 all-reduce.1
  523.5 2.1 add_convert_fusion.1
  525.7 10.3 %all-gather.16.cloned.1.call-done = bf16[256,2048]{1,0:T(8,128)(2,1)} async-done(((bf16[256,1024]{1,0:T(8,128)(2,1)}), bf16[256,2048]{1,0:T(8,128)(2,1)}) %all-gather.16.cloned.1.call-update) | async-done | bytes 1048592 | tf_op jit(solution)/shard_map/all_gather | solution.py:38
  536.0 3.9 fusion.18
  539.9 3.5 fusion.17
  543.4 3.6 collective-permute-start.1
  547.0 1.3 collective-permute-done.1
  548.4 7.0 %fusion.7 = bf16[256,2048]{1,0:T(8,128)(2,1)} fusion(bf16[2,1024,2048]{2,1,0:T(8,128)(2,1)} %all-gather.14.cloned.1.call-done, f32[2,1024]{1,0:T(2,128)S(1)} %collective-permute-done.1, f32[256,1024]{1,0:T(8,128)S(1)} %fusion.17, bf16[256,2048]{1,0:T(8,128)(2,1)S(1)} %copy-done.6, bf16[2,2048,1024]{2,1,0:T(8,128)(2,1)} %all-gather.10.cloned.1.call-done, ...), kind=kOutput, calls=%fused_computation.13 | convolution fusion | flops 2150891520 | bytes 11554816 | tf_op jit(solution)/shard_map/dot_general | solution.py:49
  555.4 10.3 %reduce-scatter.5.cloned.1.call-done = bf16[256,1024]{1,0:T(8,128)(2,1)} async-done(((bf16[256,2048]{1,0:T(8,128)(2,1)}), bf16[256,1024]{1,0:T(8,128)(2,1)}) %reduce-scatter.5.cloned.1.call-update) | async-done | bytes 524304 | tf_op jit(solution)/shard_map/reduce_scatter | solution.py:50
  565.7 1.4 fusion.35
  567.1 2.5 all-reduce
  569.6 2.1 add_convert_fusion
  (38 shorter events, 3.6 us)
Async XLA Ops:
  6.5 118.6 %all-gather.18.cloned.1.call-start = ((), (), s32[]{:S(2)}) async-start(), calls=%async_computation.9 | async-start | bytes 8912896 | tf_op jit(solution)/shard_map/all_gather | solution.py:32
  7.3 126.7 %all-gather.8.cloned.1.call-start = ((), (), s32[]{:S(2)}) async-start(), calls=%async_computation.2 | async-start | bytes 1572864 | tf_op jit(solution)/shard_map/all_gather | solution.py:38
  8.0 242.1 %all-gather.12.cloned.1.call-start = ((), (), s32[]{:S(2)}) async-start(), calls=%async_computation.4 | async-start | bytes 8912896 | tf_op jit(solution)/shard_map/all_gather | solution.py:34
  8.7 354.4 %all-gather.10.cloned.1.call-start = ((), (), s32[]{:S(2)}) async-start(), calls=%async_computation.3 | async-start | bytes 8912896 | tf_op jit(solution)/shard_map/all_gather | solution.py:33
  9.3 496.4 %all-gather.14.cloned.1.call-start = ((), (), s32[]{:S(2)}) async-start(), calls=%async_computation.5 | async-start | bytes 8912896 | tf_op jit(solution)/shard_map/all_gather | solution.py:35
  9.9 509.7 %reduce-scatter.3.cloned.1.call-start = ((), (), s32[]{:S(2)}) async-start(), calls=%async_computation.6 | async-start | bytes 1572864 | tf_op jit(solution)/shard_map/reduce_scatter | solution.py:50
  133.9 116.2 %copy-start.5 = (bf16[256,2048]{1,0:T(8,128)(2,1)S(1)}, bf16[256,2048]{1,0:T(8,128)(2,1)}, u32[]{:S(2)}) copy-start(bf16[256,2048]{1,0:T(8,128)(2,1)} %all-gather.8.cloned.1.call-done) | copy-start | bytes 3145732
  138.8 118.4 %copy-start.2 = (f32[2,3,1024]{2,0,1:T(2,128)S(1)}, f32[2,3,1024]{2,0,1:T(2,128)}, u32[]{:S(2)}) copy-start(f32[2,3,1024]{2,0,1:T(2,128)} %param.12) | copy-start | bytes 73732
  253.9 251.9 %collective-permute-start = (f32[2,1024]{1,0:T(2,128)S(1)}, f32[2,1024]{1,0:T(2,128)S(1)}, u32[]{:S(2)}, u32[]{:S(2)}) collective-permute-start(f32[2,1024]{1,0:T(2,128)S(1)} %slice.101), channel_id=1, source_target_pairs={{0,2},{2,4},{4,6},{6,8},{8,10},{10,12},{12,14},{14,16},{16,18},{18... | collective-permute-start | bytes 24584 | tf_op jit(solution)/shard_map/ppermute | solution.py:13
  505.7 7.2 %copy-start.3 = (f32[2,1024]{1,0:T(2,128)S(1)}, f32[2,1024]{1,0:T(2,128)}, u32[]{:S(2)}) copy-start(f32[2,1024]{1,0:T(2,128)} %param.14) | copy-start | bytes 24580
  505.7 7.2 %copy-start.4 = (f32[2,1024]{1,0:T(2,128)S(1)}, f32[2,1024]{1,0:T(2,128)}, u32[]{:S(2)}) copy-start(f32[2,1024]{1,0:T(2,128)} %param.15) | copy-start | bytes 24580
  505.7 13.9 %copy-start.1 = (bf16[256,1024]{1,0:T(8,128)(2,1)S(1)}, bf16[256,1024]{1,0:T(8,128)(2,1)}, u32[]{:S(2)}) copy-start(bf16[256,1024]{1,0:T(8,128)(2,1)} %param.8) | copy-start | bytes 1572868
  512.9 23.1 %all-gather.16.cloned.1.call-start = ((), (), s32[]{:S(2)}) async-start(), calls=%async_computation.7 | async-start | bytes 1572864 | tf_op jit(solution)/shard_map/all_gather | solution.py:38
  525.7 40.1 %reduce-scatter.5.cloned.1.call-start = ((), (), s32[]{:S(2)}) async-start(), calls=%async_computation.8 | async-start | bytes 1572864 | tf_op jit(solution)/shard_map/reduce_scatter | solution.py:50
  536.0 3.9 copy-start.6
  543.4 5.0 collective-permute-start.1
  548.4 17.3 %copy-start = (bf16[256,1024]{1,0:T(8,128)(2,1)S(1)}, bf16[256,1024]{1,0:T(8,128)(2,1)}, u32[]{:S(2)}) copy-start(bf16[256,1024]{1,0:T(8,128)(2,1)} %add_convert_fusion.1) | copy-start | bytes 1572868
Sparse Core Ops, SparseCore 0:
  10.1 115.0 all-gather.17
  126.7 7.1 all-gather.7
  136.7 113.3 all-gather.11
  252.7 110.3 all-gather.9
  365.7 140.0 all-gather.13
  513.0 6.5 reduce-scatter.2
  525.8 10.1 all-gather.15
  555.6 10.0 reduce-scatter.4
